TPU v7x, 32 devices: a whole 2x2x4 slice. The times are simulated.
32 devices in a mesh: grp: 2 (over y), tp: 4 (over z), dp: 4 (over x, core).
Axes of the slice: x: 2, y: 2, z: 4, core: 2. Of those that a mesh axis runs over, the one named last changes fastest.
Arguments:
- tokens: bfloat16 [64, 4096], P(('grp', 'tp'), 'dp'), parts along dimension 0, may hold values from -50 to 50
- norm_gain: float32 [2, 4096], P(None, 'dp'), may hold values from 0.1 to 1.9
- query_weight: bfloat16 [2, 4096, 4096], P(None, 'dp', 'tp'), may hold values from -0.09375 to 0.09375
- key_weight: bfloat16 [2, 4096, 4096], P(None, 'dp', 'tp'), may hold values from -0.09375 to 0.09375
- value_weight: bfloat16 [2, 4096, 4096], P(None, 'dp', 'tp'), may hold values from -0.09375 to 0.09375
- outgate_weight: bfloat16 [2, 4096, 4096], P(None, 'dp', 'tp'), may hold values from -0.09375 to 0.09375
- input_gate_weight: bfloat16 [2, 4096, 64], P(None, 'dp', 'tp'), may hold values from -0.09375 to 0.09375
- forget_gate_weight: bfloat16 [2, 4096, 64], P(None, 'dp', 'tp'), may hold values from -0.09375 to 0.09375
- forget_bias: float32 [2, 64], P(None, 'tp'), may hold values from -2 to 5
- out_weight: bfloat16 [2, 4096, 4096], P(None, 'tp', 'dp'), may hold values from -0.09375 to 0.09375
- memory_state: float32 [2, 64, 64, 4096], P(None, ('grp', 'dp'), 'tp'), parts along dimension 1, may hold values from -0.9 to 0.9
- normalizer_state: float32 [2, 64, 4096], P(None, ('grp', 'dp'), 'tp'), parts along dimension 1, may hold values from -0.9 to 0.9
- maximum_state: float32 [2, 64, 64], P(None, ('grp', 'dp'), 'tp'), parts along dimension 1, may hold values from -1 to 1
Outputs:
- next_tokens: bfloat16 [64, 4096], P(('grp', 'tp'), 'dp'), parts along dimension 0
- next_memory: float32 [2, 64, 64, 4096], P(None, ('grp', 'dp'), 'tp'), parts along dimension 1
- next_normalizer: float32 [2, 64, 4096], P(None, ('grp', 'dp'), 'tp'), parts along dimension 1
- next_maximum: float32 [2, 64, 64], P(None, ('grp', 'dp'), 'tp'), parts along dimension 1
There are 2 independent parts, one for each index of `grp`. A program takes and returns all parts, laid end to end along the dimension named above; an argument that names none is the same for every part. Nothing has to cross between parts.
All inputs are finite; a program needn't handle non-finite values.
Results may differ from a plain program's by a relative error of at most 0.0074.
Values may be sent and summed in bfloat16 or wider, within the bound.
A program may use at most 128 MiB of HBM per device.

v0:
```python
import functools

import jax
import jax.numpy as jnp
from jax import lax
from jax.experimental import pallas as pl
from jax.experimental.pallas import tpu as pltpu
from jax.sharding import PartitionSpec as P

EPS = 1e-06
F32 = jnp.float32
BF16 = jnp.bfloat16
MESH = pl.DeviceIdType.MESH
LANES = 128


def dot(a, b):
    return jnp.dot(a, b, preferred_element_type=F32)


def dot_t(a, b):
    return lax.dot_general(a, b, (((1,), (1,)), ((), ())), preferred_element_type=F32)


def iota(shape, dim):
    return lax.broadcasted_iota(jnp.int32, shape, dim)


def kernel(
    n_tp,
    n_dp,
    tokens,
    gain_in,
    wq,
    wk,
    wv,
    wg,
    wi_in,
    wf_in,
    bias_in,
    wo,
    mem_in,
    norm_in,
    max_in,
    tok_out,
    m,
    norm_out,
    max_out,
    x_all,
    gain,
    w,
    wi,
    wf,
    bias,
    norm,
    maxs,
    spread,
    fold,
    unfold,
    mask,
    p_own,
    p_send,
    p_recv,
    g_send,
    g_recv,
    mix_all,
    o_own,
    o_send,
    o_recv,
    load_sem,
    w_sem,
    m_sem,
    x_ss,
    x_rs,
    p_ss,
    p_rs,
    g_ss,
    g_rs,
    mix_ss,
    mix_rs,
    o_ss,
    o_rs,
):
    t = lax.axis_index("tp")
    d = lax.axis_index("dp")
    layers = wq.shape[0]
    rows_x, d_local = tokens.shape
    width = wq.shape[2]
    seqs, heads, square = mem_in.shape[1:]
    hd = width // heads
    hd_bits = hd.bit_length() - 1
    hp = mask.shape[0] // seqs
    rows = seqs * hp
    batch = n_tp * rows_x
    depth = d_local * n_dp
    pair = fold.shape[1]

    loads = [
        pltpu.make_async_copy(src, dst, load_sem.at[i])
        for i, (src, dst) in enumerate(
            [
                (tokens, x_all.at[0, t]),
                (gain_in, gain),
                (wi_in, wi),
                (wf_in, wf),
                (bias_in, bias),
                (max_in, maxs),
                (norm_in, norm),
            ]
        )
    ]
    for c in loads:
        c.start()
    order = (wq, wk, wv, wg, wo)
    w_loads = [
        [pltpu.make_async_copy(order[c].at[l], w.at[l, c], w_sem.at[l, c]) for c in range(5)]
        for l in range(layers)
    ]
    m_loads = [pltpu.make_async_copy(mem_in.at[l], m.at[l], m_sem.at[l]) for l in range(layers)]

    def start_loads(l, first, last):
        for c in range(first, last):
            w_loads[l][c].start()

    start_loads(0, 0, 4)
    m_loads[0].start()
    barrier = pltpu.get_barrier_semaphore()
    for o in range(1, n_tp):
        pl.semaphore_signal(
            barrier, inc=1, device_id={"tp": lax.rem(t + o, n_tp)}, device_id_type=MESH
        )
    for o in range(1, n_dp):
        pl.semaphore_signal(
            barrier, inc=1, device_id={"dp": lax.rem(d + o, n_dp)}, device_id_type=MESH
        )
    pl.semaphore_wait(barrier, n_tp + n_dp - 2)
    loads[0].wait()

    sends = []

    def send(src, dst, ss, rs, axis, peer):
        copy = pltpu.make_async_remote_copy(
            src_ref=src,
            dst_ref=dst,
            send_sem=ss,
            recv_sem=rs,
            device_id={axis: peer},
            device_id_type=MESH,
        )
        copy.start()
        sends.append(copy)
        return copy

    def send_x(l):
        return [
            send(
                x_all.at[l, t],
                x_all.at[l, t],
                x_ss.at[l, o - 1],
                x_rs.at[l, o - 1],
                "tp",
                lax.rem(t + o, n_tp),
            )
            for o in range(1, n_tp)
        ]

    x_copies = send_x(0)
    start_loads(0, 4, 5)

    spread[...] = jnp.where(
        lax.shift_right_logical(iota(spread.shape, 1), hd_bits) == iota(spread.shape, 0), 1.0, 0.0
    ).astype(BF16)
    fold[...] = jnp.where(
        (iota(fold.shape, 0) & (hd - 1)) == (iota(fold.shape, 1) & (hd - 1)), 1.0, 0.0
    ).astype(BF16)
    unfold[...] = jnp.where(
        iota(unfold.shape, 0) == (iota(unfold.shape, 1) & (hd - 1)), 1.0, 0.0
    ).astype(BF16)
    mask[...] = jnp.where(
        (iota(mask.shape, 0) & (hp - 1)) == lax.shift_right_logical(iota(mask.shape, 1), hd_bits),
        1.0,
        0.0,
    )

    def over_heads(z):
        return jnp.broadcast_to(z[:, None, :], (seqs, hp, z.shape[1])).reshape(rows, z.shape[1])

    def column(z):
        own = (iota((rows, heads), 0) & (hp - 1)) == iota((rows, heads), 1)
        return jnp.sum(jnp.where(own, over_heads(z), 0.0), axis=1, keepdims=True)

    def to_rows(z):
        return dot((over_heads(z) * mask[...]).astype(BF16), fold[...])

    def from_rows(z):
        return jnp.sum(z.reshape(seqs, hp, width), axis=1)

    def three(z):
        return z.reshape(seqs, hp, z.shape[1])[:, 0:heads]

    for c in loads[1:]:
        c.wait()

    for l in range(layers):
        for c in x_copies:
            c.wait_recv()
        x = x_all[l].astype(F32).reshape(batch, d_local)
        squares = jnp.sum(x * x, axis=1, keepdims=True)
        scaled = (x * gain[l : l + 1, :]).astype(BF16)
        g_terms = jnp.concatenate(
            [
                dot_t(scaled, wi[l]),
                dot_t(scaled, wf[l]),
                jnp.broadcast_to(squares, (batch, LANES - 2 * heads)),
            ],
            axis=1,
        )
        g_send[l] = g_terms.reshape(n_dp, seqs, LANES)
        g_copies = [
            send(
                g_send.at[l, lax.rem(d + o, n_dp)],
                g_recv.at[l, o - 1],
                g_ss.at[l, o - 1],
                g_rs.at[l, o - 1],
                "dp",
                lax.rem(d + o, n_dp),
            )
            for o in range(1, n_dp)
        ]
        p_copies = []
        for c in range(4):
            w_loads[l][c].wait()
            product = dot(scaled, w[l, c]).reshape(n_dp, seqs, width)
            p_own[c] = product
            p_send[l, c] = product.astype(BF16)
            p_copies.append(
                [
                    send(
                        p_send.at[l, c, lax.rem(d + o, n_dp)],
                        p_recv.at[l, c, o - 1],
                        p_ss.at[l, c, o - 1],
                        p_rs.at[l, c, o - 1],
                        "dp",
                        lax.rem(d + o, n_dp),
                    )
                    for o in range(1, n_dp)
                ]
            )

        if l + 1 < layers:
            start_loads(l + 1, 0, 4)
            m_loads[l + 1].start()
            start_loads(l + 1, 4, 5)

        for c in g_copies:
            c.wait_recv()
        g_sum = g_send[l, d]
        for o in range(1, n_dp):
            g_sum = g_sum + g_recv[l, o - 1]
        inv_rms = lax.rsqrt(g_sum[:, 2 * heads : 2 * heads + 1] / depth + EPS)
        input_pre = inv_rms * g_sum[:, 0:heads]
        forget_pre = inv_rms * g_sum[:, heads : 2 * heads] + bias[l : l + 1, :]
        log_forget = jnp.minimum(forget_pre, 0.0) - jnp.log1p(jnp.exp(-jnp.abs(forget_pre)))
        old_max = maxs[l]
        new_max = jnp.maximum(log_forget + old_max, input_pre)
        max_out[l] = new_max
        keep = column(jnp.exp(log_forget + old_max - new_max))
        admit = column(jnp.exp(input_pre - new_max))
        floor = column(jnp.exp(-new_max))
        if hp != heads:
            floor = jnp.where((iota((rows, 1), 0) & (hp - 1)) < heads, floor, 1.0)
        keep_wide = from_rows(keep * mask[...])
        admit_wide = from_rows(admit * mask[...])

        def stored(c):
            for copy in p_copies[c]:
                copy.wait_recv()
            total = p_own[c, d]
            for o in range(1, n_dp):
                total = total + p_recv[l, c, o - 1].astype(F32)
            return (inv_rms * total).astype(BF16).astype(F32)

        query = stored(0)
        query_rows = to_rows(query).astype(BF16)
        m_loads[l].wait()
        step = 2 * pair

        def read(j, acc):
            qx = dot(query_rows, spread[:, pl.ds(pl.multiple_of(j * step, step), step)])
            for i in range(2):
                at = pl.ds(pl.multiple_of(j * step + i * pair, pair), pair)
                acc = acc + three(qx[:, i * pair : (i + 1) * pair]) * m[l, :, :, at]
            return acc

        acc = lax.fori_loop(0, square // step, read, jnp.zeros((seqs, heads, pair), F32))
        key = stored(1) * hd ** (-0.5)
        new_norm = keep_wide * norm[l] + admit_wide * key
        norm_out[l] = new_norm
        key_rows = to_rows(key).astype(BF16)
        inner = jnp.sum(over_heads(query * new_norm) * mask[...], axis=1, keepdims=True)
        match = jnp.sum(over_heads(query * key) * mask[...], axis=1, keepdims=True)
        admitted = admit * to_rows(stored(2))
        gate = jax.nn.sigmoid(to_rows(stored(3)))
        if hp != heads:
            acc = jnp.concatenate([acc, jnp.zeros((seqs, hp - heads, pair), F32)], axis=1)
        acc = acc.reshape(rows, pair)
        acc = acc + pltpu.roll(acc, hd, 1)
        readout = (keep * acc + match * admitted) / jnp.maximum(jnp.abs(inner), floor)
        mixed = (readout * gate).astype(BF16)
        mix_all[l, d] = from_rows(dot(mixed, unfold[...]) * mask[...]).astype(BF16)
        mix_copies = [
            send(
                mix_all.at[l, d],
                mix_all.at[l, d],
                mix_ss.at[l, o - 1],
                mix_rs.at[l, o - 1],
                "dp",
                lax.rem(d + o, n_dp),
            )
            for o in range(1, n_dp)
        ]
        keep3 = three(jnp.broadcast_to(keep, (rows, pair)))
        admitted3 = three(admitted)

        @pl.loop(0, square // step)
        def update(j):
            kx = dot(key_rows, spread[:, pl.ds(pl.multiple_of(j * step, step), step)])
            for i in range(2):
                at = pl.ds(pl.multiple_of(j * step + i * pair, pair), pair)
                part = three(kx[:, i * pair : (i + 1) * pair])
                m[l, :, :, at] = keep3 * m[l, :, :, at] + part * admitted3

        w_loads[l][4].wait()
        for c in mix_copies:
            c.wait_recv()
        mixed_all = mix_all[l].astype(F32).reshape(batch, width).astype(BF16)
        partial_out = dot(mixed_all, w[l, 4]).reshape(n_tp, rows_x, d_local)
        o_own[...] = partial_out
        o_send[l] = partial_out.astype(BF16)
        o_copies = [
            send(
                o_send.at[l, lax.rem(t + o, n_tp)],
                o_recv.at[l, o - 1],
                o_ss.at[l, o - 1],
                o_rs.at[l, o - 1],
                "tp",
                lax.rem(t + o, n_tp),
            )
            for o in range(1, n_tp)
        ]
        total = o_own[t]
        for o in range(1, n_tp):
            o_copies[o - 1].wait_recv()
            total = total + o_recv[l, o - 1].astype(F32)
        result = (x_all[l, t].astype(F32) + total).astype(BF16)
        if l + 1 < layers:
            x_all[l + 1, t] = result
            x_copies = send_x(l + 1)
        else:
            tok_out[...] = result

    for c in sends:
        c.wait_send()


def store(*refs):
    n = len(refs) // 2
    copies = [pltpu.make_async_copy(refs[i], refs[n + i], refs[-1].at[i]) for i in range(n)]
    for c in copies:
        c.start()
    for c in copies:
        c.wait()


def solution(mesh):
    n_tp, n_dp = mesh.shape["tp"], mesh.shape["dp"]

    def per_device(
        tokens,
        norm_gain,
        query_weight,
        key_weight,
        value_weight,
        outgate_weight,
        input_gate_weight,
        forget_gate_weight,
        forget_bias,
        out_weight,
        memory_state,
        normalizer_state,
        maximum_state,
    ):
        rows_x, d_local = tokens.shape
        layers, _, width = query_weight.shape
        _, seqs, heads, square = memory_state.shape
        hd = width // heads
        hp = -(-heads // 8) * 8
        sem = pltpu.SemaphoreType.DMA
        vmem = pltpu.VMEM
        anywhere = pl.BlockSpec(memory_space=pl.ANY)
        in_vmem = pl.BlockSpec(memory_space=pltpu.VMEM)
        results = [
            (tokens.shape, BF16),
            (memory_state.shape, F32),
            (normalizer_state.shape, F32),
            (maximum_state.shape, F32),
        ]
        room = memory_state.size * 4 + normalizer_state.size * 4
        limit = (60 << 20) + (3 << 20) - max(room, 3 << 20) - (256 << 10)
        held = pl.pallas_call(
            functools.partial(kernel, n_tp, n_dp),
            out_shape=tuple(vmem(*r) for r in results),
            in_specs=[anywhere] * 13,
            out_specs=(in_vmem,) * 4,
            scratch_shapes=[
                vmem((layers, n_tp, rows_x, d_local), BF16),
                vmem(norm_gain.shape, F32),
                vmem((layers, 5, d_local, width), BF16),
                vmem((layers, heads, d_local), BF16),
                vmem((layers, heads, d_local), BF16),
                vmem(forget_bias.shape, F32),
                vmem(normalizer_state.shape, F32),
                vmem(maximum_state.shape, F32),
                vmem((2 * hd, square), BF16),
                vmem((width, 2 * hd), BF16),
                vmem((2 * hd, width), BF16),
                vmem((seqs * hp, width), F32),
                vmem((4, n_dp, seqs, width), F32),
                vmem((layers, 4, n_dp, seqs, width), BF16),
                vmem((layers, 4, n_dp - 1, seqs, width), BF16),
                vmem((layers, n_dp, seqs, LANES), F32),
                vmem((layers, n_dp - 1, seqs, LANES), F32),
                vmem((layers, n_dp, seqs, width), BF16),
                vmem((n_tp, rows_x, d_local), F32),
                vmem((layers, n_tp, rows_x, d_local), BF16),
                vmem((layers, n_tp - 1, rows_x, d_local), BF16),
                sem((7,)),
                sem((layers, 5)),
                sem((layers,)),
                sem((layers, n_tp - 1)),
                sem((layers, n_tp - 1)),
                sem((layers, 4, n_dp - 1)),
                sem((layers, 4, n_dp - 1)),
                sem((layers, n_dp - 1)),
                sem((layers, n_dp - 1)),
                sem((layers, n_dp - 1)),
                sem((layers, n_dp - 1)),
                sem((layers, n_tp - 1)),
                sem((layers, n_tp - 1)),
            ],
            compiler_params=pltpu.CompilerParams(
                collective_id=0, has_side_effects=True, vmem_limit_bytes=limit
            ),
        )(
            tokens,
            norm_gain,
            query_weight,
            key_weight,
            value_weight,
            outgate_weight,
            jnp.swapaxes(input_gate_weight, 1, 2),
            jnp.swapaxes(forget_gate_weight, 1, 2),
            forget_bias,
            out_weight,
            memory_state,
            normalizer_state,
            maximum_state,
        )
        return pl.pallas_call(
            store,
            out_shape=tuple(jax.ShapeDtypeStruct(*r) for r in results),
            in_specs=[in_vmem] * 4,
            out_specs=(anywhere,) * 4,
            scratch_shapes=[sem((4,))],
            compiler_params=pltpu.CompilerParams(vmem_limit_bytes=1024 * 1024),
        )(*held)

    in_specs = (
        P(("grp", "tp"), "dp"),
        P(None, "dp"),
        P(None, "dp", "tp"),
        P(None, "dp", "tp"),
        P(None, "dp", "tp"),
        P(None, "dp", "tp"),
        P(None, "dp", "tp"),
        P(None, "dp", "tp"),
        P(None, "tp"),
        P(None, "tp", "dp"),
        P(None, ("grp", "dp"), "tp", None),
        P(None, ("grp", "dp"), "tp"),
        P(None, ("grp", "dp"), "tp"),
    )
    out_specs = (
        P(("grp", "tp"), "dp"),
        P(None, ("grp", "dp"), "tp", None),
        P(None, ("grp", "dp"), "tp"),
        P(None, ("grp", "dp"), "tp"),
    )
    return jax.shard_map(
        per_device, mesh=mesh, in_specs=in_specs, out_specs=out_specs, check_vma=False
    )
```

profile of v0, /device:TPU:0, one launch (start us, length us, event | category | flops | bytes accessed | tf_op | source)
XLA Modules:
  0.0 45.5 jit_solution(7333732099216849584)
XLA Ops:
  0.6 42.8 %shard_map.156 = (bf16[8,1024]{1,0:T(8,128)(2,1)S(1)}, f32[2,8,16,4096]{3,2,1,0:T(8,128)S(1)}, f32[2,8,1024]{2,1,0:T(8,128)S(1)}, f32[2,8,16]{2,1,0:T(8,128)S(1)}) custom-call(bf16[8,1024]{1,0:T(8,128)(2,1)} %tokens.1, f32[2,1024]{1,0:T(2,128)} %gain_in.1, bf16[2,1024,1024]{2,1,0:T(8,128)(2,1)} %wq.1, bf16[2,1024,1024]{2,1,0:T(8,128)(2,1)} %wk.1, ...), custom_call_target="tpu_custom_call" | custom-call | tf_op jit(solution)/shard_map/pallas_call | solution.py:410
  43.4 2.1 %shard_map.157 = (bf16[8,1024]{1,0:T(8,128)(2,1)}, f32[2,8,16,4096]{3,2,1,0:T(8,128)}, f32[2,8,1024]{2,1,0:T(8,128)}, f32[2,8,16]{2,1,0:T(8,128)}) custom-call(bf16[8,1024]{1,0:T(8,128)(2,1)S(1)} %get-tuple-element.8.refs_0_, f32[2,8,16,4096]{3,2,1,0:T(8,128)S(1)} %get-tuple-element.9.refs_1_, f32[2,8,1024]{2,1,0:T(8,128)S(1)} %get-tuple-element.10.refs_2_, ...), custom_call_target="tpu_custom_call" | custom-call | tf_op jit(solution)/shard_map/pallas_call | solution.py:469
where the time goes:
time: 45.7 us; the launch traced here: 45.5 us
  Pallas kernels  44.8 us (98%)
  between operations  0.64 us (1%)
    pallas_call x1, Pallas kernels, per_device(): pl.pallas_call(functools.partial(kernel, n_tp, n_dp), out_shape=tuple((vm...  42.8 us
    pallas_call x1, Pallas kernels, per_device(): pl.pallas_call(store, out_shape=tuple((jax.ShapeDtypeStruct(*r) for r in...  2.06 us

commit v1 on v0

--- a/solution.py
+++ b/solution.py
@@ -292,7 +292,7 @@
                 acc = acc + three(qx[:, i * pair : (i + 1) * pair]) * m[l, :, :, at]
             return acc
 
-        acc = lax.fori_loop(0, square // step, read, jnp.zeros((seqs, heads, pair), F32))
+        acc = lax.fori_loop(0, square // step, read, jnp.zeros((seqs, heads, pair), F32), unroll=True)
         key = stored(1) * hd ** (-0.5)
         new_norm = keep_wide * norm[l] + admit_wide * key
         norm_out[l] = new_norm
@@ -322,7 +322,7 @@
         keep3 = three(jnp.broadcast_to(keep, (rows, pair)))
         admitted3 = three(admitted)
 
-        @pl.loop(0, square // step)
+        @pl.loop(0, square // step, unroll=True)
         def update(j):
             kx = dot(key_rows, spread[:, pl.ds(pl.multiple_of(j * step, step), step)])
             for i in range(2):

time: 45.7 us -> 41.4 us (0.906)
  Pallas kernels: 44.8 us -> 40.5 us
    pallas_call x1, Pallas kernels: 42.8 us -> 38.5 us  [per_device(): pl.pallas_call(functools.partial(kernel, n_tp, n_dp), out_shape=tuple((vm...]
where the time goes in v1:
time: 41.4 us; the launch traced here: 41.2 us
  Pallas kernels  40.5 us (98%)
  between operations  0.64 us (2%)
    pallas_call x1, Pallas kernels, per_device(): pl.pallas_call(functools.partial(kernel, n_tp, n_dp), out_shape=tuple((vm...  38.5 us
    pallas_call x1, Pallas kernels, per_device(): pl.pallas_call(store, out_shape=tuple((jax.ShapeDtypeStruct(*r) for r in...  2.06 us

profile of v1, /device:TPU:0, one launch (start us, length us, event | category | flops | bytes accessed | tf_op | source)
XLA Modules:
  0.0 41.2 jit_solution(16298390029827328174)
XLA Ops:
  0.6 38.5 %shard_map.156 = (bf16[8,1024]{1,0:T(8,128)(2,1)S(1)}, f32[2,8,16,4096]{3,2,1,0:T(8,128)S(1)}, f32[2,8,1024]{2,1,0:T(8,128)S(1)}, f32[2,8,16]{2,1,0:T(8,128)S(1)}) custom-call(bf16[8,1024]{1,0:T(8,128)(2,1)} %tokens.1, f32[2,1024]{1,0:T(2,128)} %gain_in.1, bf16[2,1024,1024]{2,1,0:T(8,128)(2,1)} %wq.1, bf16[2,1024,1024]{2,1,0:T(8,128)(2,1)} %wk.1, ...), custom_call_target="tpu_custom_call" | custom-call | tf_op jit(solution)/shard_map/pallas_call | solution.py:410
  39.1 2.1 %shard_map.157 = (bf16[8,1024]{1,0:T(8,128)(2,1)}, f32[2,8,16,4096]{3,2,1,0:T(8,128)}, f32[2,8,1024]{2,1,0:T(8,128)}, f32[2,8,16]{2,1,0:T(8,128)}) custom-call(bf16[8,1024]{1,0:T(8,128)(2,1)S(1)} %get-tuple-element.8.refs_0_, f32[2,8,16,4096]{3,2,1,0:T(8,128)S(1)} %get-tuple-element.9.refs_1_, f32[2,8,1024]{2,1,0:T(8,128)S(1)} %get-tuple-element.10.refs_2_, ...), custom_call_target="tpu_custom_call" | custom-call | tf_op jit(solution)/shard_map/pallas_call | solution.py:469

commit v2 on v1

v2 whole, which is shorter than its diff:
```python
import functools

import jax
import jax.numpy as jnp
from jax import lax
from jax.experimental import pallas as pl
from jax.experimental.pallas import tpu as pltpu
from jax.sharding import PartitionSpec as P

EPS = 1e-06
F32 = jnp.float32
BF16 = jnp.bfloat16
MESH = pl.DeviceIdType.MESH
LANES = 128


def dot(a, b):
    return jnp.dot(a, b, preferred_element_type=F32)


def dot_t(a, b):
    return lax.dot_general(a, b, (((1,), (1,)), ((), ())), preferred_element_type=F32)


def iota(shape, dim):
    return lax.broadcasted_iota(jnp.int32, shape, dim)


def kernel(
    n_tp,
    n_dp,
    tokens,
    gain_in,
    wq,
    wk,
    wv,
    wg,
    wi_in,
    wf_in,
    bias_in,
    wo,
    mem_in,
    norm_in,
    max_in,
    tok_out,
    m,
    norm_out,
    max_out,
    x_all,
    xs,
    gain,
    w,
    wi,
    wf,
    wif,
    bias,
    norm,
    maxs,
    spread,
    fold,
    unfold,
    mask,
    p_own,
    p_send,
    p_near,
    p_recv,
    p_pair,
    p_both,
    p_sum,
    p_far,
    g_send,
    g_recv,
    mix_all,
    o_own,
    o_send,
    o_recv,
    r_own,
    r_send,
    r_recv,
    load_sem,
    w_sem,
    m_sem,
    x_ss,
    x_rs,
    p_ss,
    p_rs,
    g_ss,
    g_rs,
    mix_ss,
    mix_rs,
    o_ss,
    o_rs,
    first_ss,
    first_rs,
    r_ss,
    r_rs,
    pair_ss,
    pair_rs,
    far_ss,
    far_rs,
):
    t = lax.axis_index("tp")
    d = lax.axis_index("dp")
    layers = wq.shape[0]
    rows_x, d_local = tokens.shape
    width = wq.shape[2]
    seqs, heads, square = mem_in.shape[1:]
    hd = width // heads
    hd_bits = hd.bit_length() - 1
    hp = mask.shape[0] // seqs
    rows = seqs * hp
    batch = n_tp * rows_x
    depth = d_local * n_dp
    pair = fold.shape[1]
    pieces = o_own.shape[0]
    cut = d_local // pieces
    spans = [slice(j * cut, (j + 1) * cut) for j in range(pieces)]

    loads = [
        pltpu.make_async_copy(src, dst, load_sem.at[i])
        for i, (src, dst) in enumerate(
            [
                (tokens, x_all.at[t]),
                (gain_in, gain),
                (wi_in, wi),
                (wf_in, wf),
                (bias_in, bias),
                (max_in, maxs),
                (norm_in, norm),
            ]
        )
    ]
    for c in loads:
        c.start()
    order = (wq, wk, wv, wg, wo)
    w_loads = [
        [pltpu.make_async_copy(order[c].at[l], w.at[l, c], w_sem.at[l, c]) for c in range(5)]
        for l in range(layers)
    ]
    m_loads = [pltpu.make_async_copy(mem_in.at[l], m.at[l], m_sem.at[l]) for l in range(layers)]

    def start_loads(l, first, last):
        for c in range(first, last):
            w_loads[l][c].start()

    start_loads(0, 0, 4)
    m_loads[0].start()
    barrier = pltpu.get_barrier_semaphore()
    for o in range(1, n_tp):
        pl.semaphore_signal(
            barrier, inc=1, device_id={"tp": lax.rem(t + o, n_tp)}, device_id_type=MESH
        )
    for o in range(1, n_dp):
        pl.semaphore_signal(
            barrier, inc=1, device_id={"dp": lax.rem(d + o, n_dp)}, device_id_type=MESH
        )
    pl.semaphore_wait(barrier, n_tp + n_dp - 2)
    loads[0].wait()

    def sibling(e):
        return e + 1 - 2 * lax.rem(e, 2)

    far = []
    for j in range(n_dp // 2):
        e = lax.rem(d + 2 * j, n_dp)
        if j:
            far.append(e)
            far.append(sibling(e))
    near = sibling(d)
    peers = far + [near]
    pairs = [2 * lax.rem(d // 2 + j, n_dp // 2) for j in range(1, n_dp // 2)]
    mine = [lax.rem(d + 2 * j, n_dp) for j in range(n_dp // 2)]
    theirs = [lax.rem(near + 2 * j, n_dp) for j in range(n_dp // 2)]
    tp_peers = [lax.rem(t + o, n_tp) for o in range(1, n_tp)]
    tp_order = tp_peers
    if n_tp % 2 == 0:
        half = n_tp // 2
        upper = t // half
        tp_order = [(1 - upper) * (n_tp - 1) + (2 * upper - 1) * j for j in range(half)]
        tp_order += [upper * half + lax.rem(t + o, half) for o in range(1, half)]

    sends = []

    def send(src, dst, ss, rs, axis, peer):
        copy = pltpu.make_async_remote_copy(
            src_ref=src,
            dst_ref=dst,
            send_sem=ss,
            recv_sem=rs,
            device_id={axis: peer},
            device_id_type=MESH,
        )
        copy.start()
        sends.append(copy)
        return copy

    def arrived(dst, ss, rs, axis, peer):
        pltpu.make_async_remote_copy(
            src_ref=dst,
            dst_ref=dst,
            send_sem=ss,
            recv_sem=rs,
            device_id={axis: peer},
            device_id_type=MESH,
        ).wait_recv()

    for o, peer in enumerate(tp_order):
        send(x_all.at[t], x_all.at[t], x_ss.at[o], x_rs.at[t], "tp", peer)
    start_loads(0, 4, 5)

    spread[...] = jnp.where(
        lax.shift_right_logical(iota(spread.shape, 1), hd_bits) == iota(spread.shape, 0), 1.0, 0.0
    ).astype(BF16)
    fold[...] = jnp.where(
        (iota(fold.shape, 0) & (hd - 1)) == (iota(fold.shape, 1) & (hd - 1)), 1.0, 0.0
    ).astype(BF16)
    unfold[...] = jnp.where(
        (iota(unfold.shape, 0) & (hd - 1)) == (iota(unfold.shape, 1) & (hd - 1)), 1.0, 0.0
    ).astype(BF16)
    mask[...] = jnp.where(
        (iota(mask.shape, 0) & (hp - 1)) == lax.shift_right_logical(iota(mask.shape, 1), hd_bits),
        1.0,
        0.0,
    )

    def over_heads(z):
        return jnp.broadcast_to(z[:, None, :], (seqs, hp, z.shape[1])).reshape(rows, z.shape[1])

    def column(z):
        own = (iota((rows, heads), 0) & (hp - 1)) == iota((rows, heads), 1)
        return jnp.sum(jnp.where(own, over_heads(z), 0.0), axis=1, keepdims=True)

    def to_rows(z):
        return dot((over_heads(z) * mask[...]).astype(BF16), fold[...])

    def from_rows(z):
        return jnp.sum(z.reshape(seqs, hp, width), axis=1)

    def three(z):
        return z.reshape(seqs, hp, z.shape[1])[:, 0:heads]

    def rounded(z):
        return z.astype(BF16).astype(F32)

    for c in loads[1:]:
        c.wait()
    for l in range(layers):
        gate_rows = jnp.concatenate(
            [
                wi[l].astype(F32),
                wf[l].astype(F32),
                jnp.zeros((LANES - 2 * heads, d_local), F32),
            ],
            axis=0,
        )
        wif[l] = gate_rows.T.astype(BF16)

    o_copies = []
    for l in range(layers):
        squares = jnp.zeros((batch, 1), F32)
        gates = jnp.zeros((batch, LANES), F32)
        p_copies = []

        def send_products(c, product):
            own = product.reshape(n_dp, seqs, width)
            p_own[l, c] = own
            if c < 2:
                p_send[l, c] = own.astype(BF16)

        def start_products(c):
            n = len(far)
            return [
                send(
                    p_send.at[l, c, peer],
                    p_recv.at[l, c, i],
                    p_ss.at[l, c, i],
                    p_rs.at[l, c, i],
                    "dp",
                    peer,
                )
                for i, peer in enumerate(far)
            ] + [
                send(
                    p_own.at[l, c, sibling(d)],
                    p_near.at[l, c],
                    p_ss.at[l, c, n],
                    p_rs.at[l, c, n],
                    "dp",
                    sibling(d),
                )
            ]

        def start_pairs(c):
            return [
                send(
                    p_own.at[l, c, e],
                    p_pair.at[l, c - 2, j],
                    pair_ss.at[l, c - 2, j],
                    pair_rs.at[l, c - 2, j],
                    "dp",
                    near,
                )
                for j, e in enumerate(theirs)
            ]

        def pass_pairs(c):
            for copy in p_copies[c]:
                copy.wait_recv()
            p_both[c - 2] = p_own[l, c, d] + p_pair[l, c - 2, 0]
            copies = []
            for j in range(1, n_dp // 2):
                p_sum[l, c - 2, j - 1] = (p_own[l, c, mine[j]] + p_pair[l, c - 2, j]).astype(BF16)
                copies.append(
                    send(
                        p_sum.at[l, c - 2, j - 1],
                        p_far.at[l, c - 2, j - 1],
                        far_ss.at[l, c - 2, j - 1],
                        far_rs.at[l, c - 2, j - 1],
                        "dp",
                        mine[j],
                    )
                )
            return copies

        steps = spans if l else [slice(0, d_local)]
        for j, span in enumerate(steps):
            if l == 0:
                for peer in tp_peers:
                    arrived(x_all.at[peer], x_ss.at[0], x_rs.at[peer], "tp", peer)
                x = x_all[...].astype(F32).reshape(batch, d_local)
            else:
                total = o_own[j]
                for copy in o_first if j == 0 else []:
                    copy.wait_recv()
                for copy in o_copies[j]:
                    copy.wait_recv()
                for o in range(n_tp - 1):
                    total = total + o_recv[l - 1, o, j].astype(F32)
                total = total.reshape(batch, cut)
                x = rounded(xs[:, span] + total)
            xs[:, span] = x
            squares = squares + jnp.sum(x * x, axis=1, keepdims=True)
            scaled = (x * gain[l : l + 1, span]).astype(BF16)
            gates = gates + dot(scaled, wif[l, span])
            if j == 0:
                for c in range(4):
                    w_loads[l][c].wait()

            def project(c):
                product = dot(scaled, w[l, c, span])
                if j:
                    product = product + p_own[l, c].reshape(batch, width)
                return product

            if j + 1 < len(steps):
                for c in range(4):
                    p_own[l, c] = project(c).reshape(n_dp, seqs, width)
                continue
            ahead = project(0)
            g_send[l] = jnp.where(iota((batch, LANES), 1) < 2 * heads, gates, squares).reshape(
                n_dp, seqs, LANES
            )
            for c in range(4):
                product, ahead = ahead, project(c + 1) if c < 3 else None
                send_products(c, product)
                if c == 0:
                    g_copies = [
                        send(
                            g_send.at[l, peer],
                            g_recv.at[l, i],
                            g_ss.at[l, i],
                            g_rs.at[l, i],
                            "dp",
                            peer,
                        )
                        for i, peer in enumerate(peers)
                    ]
                p_copies.append(start_products(c) if c < 2 else start_pairs(c))

        far_copies = [pass_pairs(c) for c in (2, 3)]

        if l + 1 < layers:
            start_loads(l + 1, 0, 4)
            m_loads[l + 1].start()
            start_loads(l + 1, 4, 5)

        for c in g_copies:
            c.wait_recv()
        g_sum = g_send[l, d]
        for i in range(n_dp - 1):
            g_sum = g_sum + g_recv[l, i]
        inv_rms = lax.rsqrt(g_sum[:, 2 * heads : 2 * heads + 1] / depth + EPS)
        input_pre = inv_rms * g_sum[:, 0:heads]
        forget_pre = inv_rms * g_sum[:, heads : 2 * heads] + bias[l : l + 1, :]
        log_forget = jnp.minimum(forget_pre, 0.0) - jnp.log1p(jnp.exp(-jnp.abs(forget_pre)))
        old_max = maxs[l]
        new_max = jnp.maximum(log_forget + old_max, input_pre)
        max_out[l] = new_max
        keep = column(jnp.exp(log_forget + old_max - new_max))
        admit = column(jnp.exp(input_pre - new_max))
        floor = column(jnp.exp(-new_max))
        if hp != heads:
            floor = jnp.where((iota((rows, 1), 0) & (hp - 1)) < heads, floor, 1.0)

        def stored(c):
            for copy in p_copies[c]:
                copy.wait_recv()
            total = p_own[l, c, d] + p_near[l, c]
            for i in range(n_dp - 2):
                total = total + p_recv[l, c, i].astype(F32)
            return rounded(inv_rms * total)

        def stored_pair(c):
            total = p_both[c - 2]
            for j, copy in enumerate(far_copies[c - 2]):
                copy.wait_recv()
                total = total + p_far[l, c - 2, j].astype(F32)
            return rounded(inv_rms * total)

        query = stored(0)
        m_loads[l].wait()
        query_rows = to_rows(query)
        query_low = query_rows.astype(BF16)
        old_inner = jnp.sum(over_heads(query * norm[l]) * mask[...], axis=1, keepdims=True)
        step = 2 * pair

        acc = jnp.zeros((seqs, heads, pair), F32)
        for j in range(square // step):
            qx = dot(query_low, spread[:, j * step : (j + 1) * step])
            for i in range(2):
                at = slice(j * step + i * pair, j * step + (i + 1) * pair)
                acc = acc + three(qx[:, i * pair : (i + 1) * pair]) * m[l, :, :, at]
        if hp != heads:
            acc = jnp.concatenate([acc, jnp.zeros((seqs, hp - heads, pair), F32)], axis=1)
        acc = acc.reshape(rows, pair)
        acc = acc + pltpu.roll(acc, hd, 1)

        key = stored(1) * hd ** (-0.5)
        key_rows = to_rows(key)
        match = jnp.sum(query_rows * key_rows, axis=1, keepdims=True) * (hd / pair)
        inner = keep * old_inner + admit * match
        bound = jnp.maximum(jnp.abs(inner), floor)
        fresh = match * admit / bound
        past = keep * acc / bound
        top = rounded(past)
        halves = jnp.where(iota((rows, pair), 1) < hd, top, past - top).astype(BF16)
        past_wide = from_rows(dot(halves, unfold[...]) * mask[...])
        fresh_wide = from_rows(fresh * mask[...])
        value = stored_pair(2)
        readout = past_wide + fresh_wide * value
        mix_all[l, d] = (readout * jax.nn.sigmoid(stored_pair(3))).astype(BF16)
        mix_copies = [
            send(
                mix_all.at[l, d],
                mix_all.at[l, d],
                mix_ss.at[l, i],
                mix_rs.at[l, i],
                "dp",
                peer,
            )
            for i, peer in enumerate(peers)
        ]
        w_loads[l][4].wait()
        if l + 1 < layers:
            o_first = []
            for i, e in enumerate((d, near)):
                if i:
                    mix_copies[-1].wait_recv()
                partial_out = dot(mix_all[l, e], w[l, 4])
                for j, span in enumerate(spans):
                    o_own[j, e] = partial_out[:, span]
                    o_send[l, j, e] = partial_out[:, span].astype(BF16)
                for o, peer in enumerate(tp_peers):
                    o_first.append(
                        send(
                            o_send.at[l, :, e],
                            o_recv.at[l, o, :, e],
                            first_ss.at[l, i, o],
                            first_rs.at[l, i, o],
                            "tp",
                            peer,
                        )
                    )
        norm_out[l] = from_rows(keep * mask[...]) * norm[l] + from_rows(admit * mask[...]) * key
        keep3 = three(jnp.broadcast_to(keep, (rows, pair)))
        admitted3 = three(admit * to_rows(value))
        key_low = key_rows.astype(BF16)

        for j in range(square // step):
            kx = dot(key_low, spread[:, j * step : (j + 1) * step])
            for i in range(2):
                at = slice(j * step + i * pair, j * step + (i + 1) * pair)
                part = three(kx[:, i * pair : (i + 1) * pair])
                m[l, :, :, at] = keep3 * m[l, :, :, at] + part * admitted3

        for c in mix_copies[: n_dp - 2 if l + 1 < layers else n_dp - 1]:
            c.wait_recv()
        if l + 1 < layers:
            mixed = [
                mix_all[l, pl.ds(e, 2)].astype(F32).reshape(2 * seqs, width).astype(BF16)
                for e in pairs
            ]
            o_copies = []
            for j, span in enumerate(spans):
                o_copies.append([])
                for i, e in enumerate(pairs):
                    partial_out = dot(mixed[i], w[l, 4, :, span]).reshape(2, seqs, cut)
                    o_own[j, pl.ds(e, 2)] = partial_out
                    o_send[l, j, pl.ds(e, 2)] = partial_out.astype(BF16)
                    for o, peer in enumerate(tp_peers):
                        o_copies[j].append(
                            send(
                                o_send.at[l, j, pl.ds(e, 2)],
                                o_recv.at[l, o, j, pl.ds(e, 2)],
                                o_ss.at[l, j, i, o],
                                o_rs.at[l, j, i, o],
                                "tp",
                                peer,
                            )
                        )
        else:
            mixed_all = mix_all[l].astype(F32).reshape(batch, width).astype(BF16)
            partial_out = dot(mixed_all, w[l, 4]).reshape(n_tp, rows_x, d_local)
            r_own[...] = partial_out
            r_send[...] = partial_out.astype(BF16)
            for o, peer in enumerate(tp_order):
                send(r_send.at[peer], r_recv.at[t], r_ss.at[o], r_rs.at[t], "tp", peer)
            total = r_own[t]
            for peer in tp_peers:
                arrived(r_recv.at[peer], r_ss.at[0], r_rs.at[peer], "tp", peer)
            for peer in tp_peers:
                total = total + r_recv[peer].astype(F32)
            own_rows = pl.ds(pl.multiple_of(t * rows_x, rows_x), rows_x)
            tok_out[...] = (xs[own_rows, :] + total).astype(BF16)

    for c in sends:
        c.wait_send()


def store(*refs):
    n = len(refs) // 2
    copies = [pltpu.make_async_copy(refs[i], refs[n + i], refs[-1].at[i]) for i in range(n)]
    for c in copies:
        c.start()
    for c in copies:
        c.wait()


def solution(mesh):
    n_tp, n_dp = mesh.shape["tp"], mesh.shape["dp"]

    def per_device(
        tokens,
        norm_gain,
        query_weight,
        key_weight,
        value_weight,
        outgate_weight,
        input_gate_weight,
        forget_gate_weight,
        forget_bias,
        out_weight,
        memory_state,
        normalizer_state,
        maximum_state,
    ):
        rows_x, d_local = tokens.shape
        layers, _, width = query_weight.shape
        _, seqs, heads, square = memory_state.shape
        hd = width // heads
        hp = -(-heads // 8) * 8
        batch = n_tp * rows_x
        pieces = 4 if d_local % 512 == 0 else 1
        sem = pltpu.SemaphoreType.DMA
        vmem = pltpu.VMEM
        anywhere = pl.BlockSpec(memory_space=pl.ANY)
        in_vmem = pl.BlockSpec(memory_space=pltpu.VMEM)
        results = [
            (tokens.shape, BF16),
            (memory_state.shape, F32),
            (normalizer_state.shape, F32),
            (maximum_state.shape, F32),
        ]
        room = memory_state.size * 4 + normalizer_state.size * 4
        limit = (60 << 20) + (3 << 20) - max(room, 3 << 20) - (256 << 10)
        held = pl.pallas_call(
            functools.partial(kernel, n_tp, n_dp),
            out_shape=tuple(vmem(*r) for r in results),
            in_specs=[anywhere] * 13,
            out_specs=(in_vmem,) * 4,
            scratch_shapes=[
                vmem((n_tp, rows_x, d_local), BF16),
                vmem((batch, d_local), F32),
                vmem(norm_gain.shape, F32),
                vmem((layers, 5, d_local, width), BF16),
                vmem((layers, heads, d_local), BF16),
                vmem((layers, heads, d_local), BF16),
                vmem((layers, d_local, LANES), BF16),
                vmem(forget_bias.shape, F32),
                vmem(normalizer_state.shape, F32),
                vmem(maximum_state.shape, F32),
                vmem((2 * hd, square), BF16),
                vmem((width, 2 * hd), BF16),
                vmem((2 * hd, width), BF16),
                vmem((seqs * hp, width), F32),
                vmem((layers, 4, n_dp, seqs, width), F32),
                vmem((layers, 2, n_dp, seqs, width), BF16),
                vmem((layers, 2, seqs, width), F32),
                vmem((layers, 2, n_dp - 2, seqs, width), BF16),
                vmem((layers, 2, n_dp // 2, seqs, width), F32),
                vmem((2, seqs, width), F32),
                vmem((layers, 2, n_dp // 2 - 1, seqs, width), BF16),
                vmem((layers, 2, n_dp // 2 - 1, seqs, width), BF16),
                vmem((layers, n_dp, seqs, LANES), F32),
                vmem((layers, n_dp - 1, seqs, LANES), F32),
                vmem((layers, n_dp, seqs, width), BF16),
                vmem((pieces, n_dp, seqs, d_local // pieces), F32),
                vmem((layers - 1, pieces, n_dp, seqs, d_local // pieces), BF16),
                vmem((layers - 1, n_tp - 1, pieces, n_dp, seqs, d_local // pieces), BF16),
                vmem((n_tp, rows_x, d_local), F32),
                vmem((n_tp, rows_x, d_local), BF16),
                vmem((n_tp, rows_x, d_local), BF16),
                sem((7,)),
                sem((layers, 5)),
                sem((layers,)),
                sem((n_tp - 1,)),
                sem((n_tp,)),
                sem((layers, 2, n_dp - 1)),
                sem((layers, 2, n_dp - 1)),
                sem((layers, n_dp - 1)),
                sem((layers, n_dp - 1)),
                sem((layers, n_dp - 1)),
                sem((layers, n_dp - 1)),
                sem((layers - 1, pieces, n_dp // 2 - 1, n_tp - 1)),
                sem((layers - 1, pieces, n_dp // 2 - 1, n_tp - 1)),
                sem((layers - 1, 2, n_tp - 1)),
                sem((layers - 1, 2, n_tp - 1)),
                sem((n_tp - 1,)),
                sem((n_tp,)),
                sem((layers, 2, n_dp // 2)),
                sem((layers, 2, n_dp // 2)),
                sem((layers, 2, n_dp // 2 - 1)),
                sem((layers, 2, n_dp // 2 - 1)),
            ],
            compiler_params=pltpu.CompilerParams(
                collective_id=0, has_side_effects=True, vmem_limit_bytes=limit
            ),
        )(
            tokens,
            norm_gain,
            query_weight,
            key_weight,
            value_weight,
            outgate_weight,
            jnp.swapaxes(input_gate_weight, 1, 2),
            jnp.swapaxes(forget_gate_weight, 1, 2),
            forget_bias,
            out_weight,
            memory_state,
            normalizer_state,
            maximum_state,
        )
        return pl.pallas_call(
            store,
            out_shape=tuple(jax.ShapeDtypeStruct(*r) for r in results),
            in_specs=[in_vmem] * 4,
            out_specs=(anywhere,) * 4,
            scratch_shapes=[sem((4,))],
            compiler_params=pltpu.CompilerParams(vmem_limit_bytes=1024 * 1024),
        )(*held)

    in_specs = (
        P(("grp", "tp"), "dp"),
        P(None, "dp"),
        P(None, "dp", "tp"),
        P(None, "dp", "tp"),
        P(None, "dp", "tp"),
        P(None, "dp", "tp"),
        P(None, "dp", "tp"),
        P(None, "dp", "tp"),
        P(None, "tp"),
        P(None, "tp", "dp"),
        P(None, ("grp", "dp"), "tp", None),
        P(None, ("grp", "dp"), "tp"),
        P(None, ("grp", "dp"), "tp"),
    )
    out_specs = (
        P(("grp", "tp"), "dp"),
        P(None, ("grp", "dp"), "tp", None),
        P(None, ("grp", "dp"), "tp"),
        P(None, ("grp", "dp"), "tp"),
    )
    return jax.shard_map(
        per_device, mesh=mesh, in_specs=in_specs, out_specs=out_specs, check_vma=False
    )
```

time: 41.4 us -> 38.1 us (0.920)
  Pallas kernels: 40.5 us -> 37.3 us
    pallas_call x1, Pallas kernels: 38.5 us -> 35.2 us  [per_device(): pl.pallas_call(functools.partial(kernel, n_tp, n_dp), out_shape=tuple((vm...]
where the time goes in v2:
time: 38.1 us; the launch traced here: 37.9 us
  Pallas kernels  37.3 us (98%)
  between operations  0.64 us (2%)
    pallas_call x1, Pallas kernels, per_device(): pl.pallas_call(functools.partial(kernel, n_tp, n_dp), out_shape=tuple((vm...  35.2 us
    pallas_call x1, Pallas kernels, per_device(): pl.pallas_call(store, out_shape=tuple((jax.ShapeDtypeStruct(*r) for r in...  2.06 us

profile of v2, /device:TPU:0, one launch (start us, length us, event | category | flops | bytes accessed | tf_op | source)
XLA Modules:
  0.0 37.9 jit_solution(12115337745513867939)
XLA Ops:
  0.6 35.2 %shard_map.156 = (bf16[8,1024]{1,0:T(8,128)(2,1)S(1)}, f32[2,8,16,4096]{3,2,1,0:T(8,128)S(1)}, f32[2,8,1024]{2,1,0:T(8,128)S(1)}, f32[2,8,16]{2,1,0:T(8,128)S(1)}) custom-call(bf16[8,1024]{1,0:T(8,128)(2,1)} %tokens.1, f32[2,1024]{1,0:T(2,128)} %gain_in.1, bf16[2,1024,1024]{2,1,0:T(8,128)(2,1)} %wq.1, bf16[2,1024,1024]{2,1,0:T(8,128)(2,1)} %wk.1, ...), custom_call_target="tpu_custom_call" | custom-call | tf_op jit(solution)/shard_map/pallas_call | solution.py:586
  35.9 2.1 %shard_map.157 = (bf16[8,1024]{1,0:T(8,128)(2,1)}, f32[2,8,16,4096]{3,2,1,0:T(8,128)}, f32[2,8,1024]{2,1,0:T(8,128)}, f32[2,8,16]{2,1,0:T(8,128)}) custom-call(bf16[8,1024]{1,0:T(8,128)(2,1)S(1)} %get-tuple-element.8.refs_0_, f32[2,8,16,4096]{3,2,1,0:T(8,128)S(1)} %get-tuple-element.9.refs_1_, f32[2,8,1024]{2,1,0:T(8,128)S(1)} %get-tuple-element.10.refs_2_, ...), custom_call_target="tpu_custom_call" | custom-call | tf_op jit(solution)/shard_map/pallas_call | solution.py:663

commit v3 on v2

--- a/solution.py
+++ b/solution.py
@@ -169,8 +169,8 @@
     near = sibling(d)
     peers = far + [near]
     pairs = [2 * lax.rem(d // 2 + j, n_dp // 2) for j in range(1, n_dp // 2)]
-    mine = [lax.rem(d + 2 * j, n_dp) for j in range(n_dp // 2)]
-    theirs = [lax.rem(near + 2 * j, n_dp) for j in range(n_dp // 2)]
+    theirs = [near] + [lax.rem(d + 2 * j, n_dp) for j in range(1, n_dp // 2)]
+    mine = [d] + [sibling(e) for e in theirs[1:]]
     tp_peers = [lax.rem(t + o, n_tp) for o in range(1, n_tp)]
     tp_order = tp_peers
     if n_tp % 2 == 0:
@@ -207,6 +207,10 @@
     for o, peer in enumerate(tp_order):
         send(x_all.at[t], x_all.at[t], x_ss.at[o], x_rs.at[t], "tp", peer)
     start_loads(0, 4, 5)
+    for l in range(1, layers):
+        start_loads(l, 0, 4)
+        m_loads[l].start()
+        start_loads(l, 4, 5)
 
     spread[...] = jnp.where(
         lax.shift_right_logical(iota(spread.shape, 1), hd_bits) == iota(spread.shape, 0), 1.0, 0.0
@@ -378,11 +382,6 @@
                 p_copies.append(start_products(c) if c < 2 else start_pairs(c))
 
         far_copies = [pass_pairs(c) for c in (2, 3)]
-
-        if l + 1 < layers:
-            start_loads(l + 1, 0, 4)
-            m_loads[l + 1].start()
-            start_loads(l + 1, 4, 5)
 
         for c in g_copies:
             c.wait_recv()
@@ -470,7 +469,8 @@
                 for j, span in enumerate(spans):
                     o_own[j, e] = partial_out[:, span]
                     o_send[l, j, e] = partial_out[:, span].astype(BF16)
-                for o, peer in enumerate(tp_peers):
+                for o in (1, 0, 2):
+                    peer = tp_peers[o]
                     o_first.append(
                         send(
                             o_send.at[l, :, e],
@@ -507,7 +507,8 @@
                     partial_out = dot(mixed[i], w[l, 4, :, span]).reshape(2, seqs, cut)
                     o_own[j, pl.ds(e, 2)] = partial_out
                     o_send[l, j, pl.ds(e, 2)] = partial_out.astype(BF16)
-                    for o, peer in enumerate(tp_peers):
+                    for o in (1, 0, 2):
+                        peer = tp_peers[o]
                         o_copies[j].append(
                             send(
                                 o_send.at[l, j, pl.ds(e, 2)],
@@ -525,6 +526,8 @@
             r_send[...] = partial_out.astype(BF16)
             for o, peer in enumerate(tp_order):
                 send(r_send.at[peer], r_recv.at[t], r_ss.at[o], r_rs.at[t], "tp", peer)
+            for c in sends[: 1 - n_tp]:
+                c.wait_send()
             total = r_own[t]
             for peer in tp_peers:
                 arrived(r_recv.at[peer], r_ss.at[0], r_rs.at[peer], "tp", peer)
@@ -533,7 +536,7 @@
             own_rows = pl.ds(pl.multiple_of(t * rows_x, rows_x), rows_x)
             tok_out[...] = (xs[own_rows, :] + total).astype(BF16)
 
-    for c in sends:
+    for c in sends[1 - n_tp :]:
         c.wait_send()
 
 

time: 38.1 us -> 37.8 us (level)
  no operation moved by 1% of the time
where the time goes in v3:
time: 37.8 us; the launch traced here: 37.6 us
  Pallas kernels  37 us (98%)
  between operations  0.64 us (2%)
    pallas_call x1, Pallas kernels, per_device(): pl.pallas_call(functools.partial(kernel, n_tp, n_dp), out_shape=tuple((vm...  34.9 us
    pallas_call x1, Pallas kernels, per_device(): pl.pallas_call(store, out_shape=tuple((jax.ShapeDtypeStruct(*r) for r in...  2.06 us

profile of v3, /device:TPU:0, one launch (start us, length us, event | category | flops | bytes accessed | tf_op | source)
XLA Modules:
  0.0 37.6 jit_solution(2817542294729173637)
XLA Ops:
  0.6 34.9 %shard_map.156 = (bf16[8,1024]{1,0:T(8,128)(2,1)S(1)}, f32[2,8,16,4096]{3,2,1,0:T(8,128)S(1)}, f32[2,8,1024]{2,1,0:T(8,128)S(1)}, f32[2,8,16]{2,1,0:T(8,128)S(1)}) custom-call(bf16[8,1024]{1,0:T(8,128)(2,1)} %tokens.1, f32[2,1024]{1,0:T(2,128)} %gain_in.1, bf16[2,1024,1024]{2,1,0:T(8,128)(2,1)} %wq.1, bf16[2,1024,1024]{2,1,0:T(8,128)(2,1)} %wk.1, ...), custom_call_target="tpu_custom_call" | custom-call | tf_op jit(solution)/shard_map/pallas_call | solution.py:589
  35.6 2.1 %shard_map.157 = (bf16[8,1024]{1,0:T(8,128)(2,1)}, f32[2,8,16,4096]{3,2,1,0:T(8,128)}, f32[2,8,1024]{2,1,0:T(8,128)}, f32[2,8,16]{2,1,0:T(8,128)}) custom-call(bf16[8,1024]{1,0:T(8,128)(2,1)S(1)} %get-tuple-element.8.refs_0_, f32[2,8,16,4096]{3,2,1,0:T(8,128)S(1)} %get-tuple-element.9.refs_1_, f32[2,8,1024]{2,1,0:T(8,128)S(1)} %get-tuple-element.10.refs_2_, ...), custom_call_target="tpu_custom_call" | custom-call | tf_op jit(solution)/shard_map/pallas_call | solution.py:666
